TPU v7x, 32 devices: a whole 2x2x4 slice. The times are simulated.
32 devices in a mesh: sp: 8 (over z, x), tp: 4 (over y, core).
Axes of the slice: x: 2, y: 2, z: 4, core: 2. Of those that a mesh axis runs over, the one named last changes fastest.
Arguments:
- residual: bfloat16 [8192, 2048], P('sp'), may hold values from -6 to 6
- query: bfloat16 [8192, 1024], P('sp', 'tp'), may hold values from -6 to 6
- key: bfloat16 [8192, 256], P('sp', 'tp'), may hold values from -6 to 6
- value: bfloat16 [8192, 256], P('sp', 'tp'), may hold values from -6 to 6
- sink: float32 [16], P('tp'), may hold values from 3 to 9
- norm_gain: float32 [2048], replicated, may hold values from 0.1 to 1.9
- w_out: bfloat16 [1024, 2048], P('tp'), may hold values from -1.5 to 1.5
- w_gate: bfloat16 [2048, 4096], P('sp', 'tp'), may hold values from -0.125 to 0.125
- w_value: bfloat16 [2048, 4096], P('sp', 'tp'), may hold values from -0.125 to 0.125
- conv_gate: bfloat16 [3, 4096], P(None, 'tp'), may hold values from -3 to 3
- conv_value: bfloat16 [3, 4096], P(None, 'tp'), may hold values from -3 to 3
- w_down: bfloat16 [4096, 2048], P('tp', 'sp'), may hold values from -0.09375 to 0.09375
Outputs:
- layer_out: bfloat16 [8192, 2048], P(('sp', 'tp'))
All inputs are finite; a program needn't handle non-finite values.
Results may differ from a plain program's by a relative error of at most 0.015.
Values may be sent and summed in bfloat16 or wider, within the bound.
A program may use at most 128 MiB of HBM per device.

v0:
```python
import jax
import jax.numpy as jnp
from jax import lax
from jax.sharding import PartitionSpec as P

HD = 64
WINDOW = 128
THETA = 10000.0
EPS = 1e-06


def extended(block, sides, width):
    for axis, dim in sides:
        count = lax.axis_size(axis)
        forward = [(i, i + 1) for i in range(count - 1)]
        backward = [(target, source) for source, target in forward]
        low = lax.ppermute(
            lax.slice_in_dim(block, block.shape[dim] - width, None, axis=dim), axis, forward
        )
        high = lax.ppermute(lax.slice_in_dim(block, 0, width, axis=dim), axis, backward)
        block = jnp.concatenate([low, block, high], axis=dim)
    return block


def rotate(field, positions):
    count = field.shape[0]
    parts = field.astype(jnp.float32).reshape(count, -1, HD)
    inverse = 1.0 / THETA ** (jnp.arange(0, HD, 2, dtype=jnp.float32) / HD)
    angle = positions[:, None] * inverse[None, :]
    cosine = jnp.cos(angle)[:, None, :]
    sine = jnp.sin(angle)[:, None, :]
    first = parts[..., : HD // 2]
    second = parts[..., HD // 2 :]
    turned = jnp.concatenate(
        [first * cosine - second * sine, second * cosine + first * sine], axis=-1
    )
    return turned.reshape(count, -1).astype(jnp.bfloat16)


def band_attention(queries, keys, values, sinks, start, total):
    count = queries.shape[0]
    blocks = count // WINDOW
    kv_local = keys.shape[1] // HD
    group = queries.shape[1] // (kv_local * HD)
    query_blocks = queries.reshape(blocks, WINDOW, kv_local, group, HD)
    key_band = jnp.concatenate(
        [
            keys[i * WINDOW : i * WINDOW + count].reshape(blocks, WINDOW, kv_local, HD)
            for i in range(3)
        ],
        axis=1,
    )
    value_band = jnp.concatenate(
        [
            values[i * WINDOW : i * WINDOW + count].reshape(blocks, WINDOW, kv_local, HD)
            for i in range(3)
        ],
        axis=1,
    )
    scores = jnp.einsum(
        "nqkgd,njkd->nkgqj", query_blocks, key_band, preferred_element_type=jnp.float32
    ) * HD ** (-0.5)
    block_ids = jnp.arange(blocks, dtype=jnp.int32)[:, None]
    query_pos = start + block_ids * WINDOW + jnp.arange(WINDOW, dtype=jnp.int32)[None, :]
    key_pos = start - WINDOW + block_ids * WINDOW + jnp.arange(3 * WINDOW, dtype=jnp.int32)[None, :]
    valid = (
        (key_pos[:, None, :] >= 0)
        & (key_pos[:, None, :] < total)
        & (jnp.abs(query_pos[:, :, None] - key_pos[:, None, :]) <= WINDOW)
    )
    scores = jnp.where(valid[:, None, None], scores, -1e30)
    sink_col = sinks.reshape(1, kv_local, group, 1, 1)
    top = jnp.maximum(jnp.max(scores, axis=-1, keepdims=True), sink_col)
    weights = jnp.exp(scores - top)
    denom = jnp.sum(weights, axis=-1, keepdims=True) + jnp.exp(sink_col - top)
    probs = (weights / denom).astype(jnp.bfloat16)
    out = jnp.einsum("nkgqj,njkd->nqkgd", probs, value_band, preferred_element_type=jnp.float32)
    return out.reshape(count, kv_local * group * HD).astype(jnp.bfloat16)


def rmsnorm(field, gain):
    wide = field.astype(jnp.float32)
    scale = lax.rsqrt(jnp.mean(wide * wide, axis=-1, keepdims=True) + EPS)
    return (wide * scale * gain).astype(jnp.bfloat16)


def shards(
    residual,
    query,
    key,
    value,
    sink,
    norm_gain,
    w_out,
    w_gate,
    w_value,
    conv_gate,
    conv_value,
    w_down,
):
    tok_rows = query.shape[0]
    offset = lax.axis_index("sp") * tok_rows
    total = tok_rows * lax.axis_size("sp")
    share = tok_rows // lax.axis_size("tp")
    tp_index = lax.axis_index("tp")
    positions = (offset + jnp.arange(tok_rows, dtype=jnp.int32)).astype(jnp.float32)
    turned_query = rotate(query, positions)
    turned_key = rotate(key, positions)
    key_width = key.shape[1]
    band = jnp.concatenate([turned_key, value], axis=1)
    edged = extended(band, (("sp", 0),), WINDOW)
    attended = band_attention(
        turned_query, edged[:, :key_width], edged[:, key_width:], sink, offset, total
    )
    partial_value = jnp.dot(attended, w_out, preferred_element_type=jnp.float32)
    mix_full = lax.psum(partial_value.astype(jnp.bfloat16), "tp").astype(jnp.float32)
    mid_full = (residual.astype(jnp.float32) + mix_full).astype(jnp.bfloat16)
    normed = rmsnorm(mid_full, norm_gain)
    mid_rows = lax.dynamic_slice_in_dim(mid_full, tp_index * share, share, 0)
    gate_full, value_full = (
        lax.all_gather(w_gate, "sp", axis=0, tiled=True),
        lax.all_gather(w_value, "sp", axis=0, tiled=True),
    )
    gate_up = jnp.dot(normed, gate_full, preferred_element_type=jnp.float32).astype(jnp.bfloat16)
    value_up = jnp.dot(normed, value_full, preferred_element_type=jnp.float32).astype(jnp.bfloat16)
    hidden_width = gate_up.shape[1]
    stacked = jnp.concatenate([gate_up, value_up], axis=1)
    edged_up = extended(stacked, (("sp", 0),), 1).astype(jnp.float32)
    taps = jnp.concatenate([conv_gate, conv_value], axis=1).astype(jnp.float32)
    convolved = edged_up[:-2] * taps[0] + edged_up[1:-1] * taps[1] + edged_up[2:] * taps[2]
    hidden = (jax.nn.silu(convolved[:, :hidden_width]) * convolved[:, hidden_width:]).astype(
        jnp.bfloat16
    )
    terms = jnp.dot(
        hidden, lax.all_gather(w_down, "sp", axis=1, tiled=True), preferred_element_type=jnp.float32
    )
    ffn_rows = lax.psum_scatter(
        terms.astype(jnp.bfloat16), "tp", scatter_dimension=0, tiled=True
    ).astype(jnp.float32)
    return (mid_rows.astype(jnp.float32) + ffn_rows).astype(jnp.bfloat16)


def solution(mesh):
    return jax.shard_map(
        shards,
        mesh=mesh,
        in_specs=(
            P("sp", None),
            P("sp", "tp"),
            P("sp", "tp"),
            P("sp", "tp"),
            P("tp"),
            P(),
            P("tp", None),
            P("sp", "tp"),
            P("sp", "tp"),
            P(None, "tp"),
            P(None, "tp"),
            P("tp", "sp"),
        ),
        out_specs=P(("sp", "tp"), None),
        check_vma=False,
    )
```

profile of v0, /device:TPU:0, one launch (start us, length us, event | category | flops | bytes accessed | tf_op | source)
XLA Modules:
  0.0 336.9 jit_solution(1129287583386971566)
XLA Ops:
  7.4 1.0 bitcast_convert_fusion
  8.4 0.6 fusion.40
  9.0 0.8 pad_maximum_fusion.6
  9.8 4.9 %collective-permute-start = (bf16[128,128]{0,1:T(8,128)(2,1)S(1)}, bf16[128,128]{0,1:T(8,128)(2,1)S(1)}, u32[]{:S(2)}, u32[]{:S(2)}) collective-permute-start(bf16[128,128]{0,1:T(8,128)(2,1)S(1)} %get-tuple-element.19), channel_id=1, source_target_pairs={{0,4},{4,8},{8,12},{12,16},{16,20},{20,24},{24,28},{1,5},{5,9},{9,... | collective-permute-start | bytes 98312 | tf_op jit(solution)/shard_map/ppermute | solution.py:17
  14.7 1.3 collective-permute-start.1
  16.0 0.5 multiply_cosine_fusion
  16.7 1.2 copy.20
  18.3 1.2 fusion.12
  19.5 0.9 collective-permute-done.1
  20.7 1.0 fusion.6
  21.8 1.5 fusion.5
  23.5 1.9 fusion.16
  25.8 3.3 convolution_convert_fusion
  29.2 0.5 all-gather.6.cloned.1.call-update
  29.7 0.5 all-gather.4.cloned.1.call-update
  30.3 0.5 all-gather.8.cloned.1.call-update
  31.2 85.1 %all-reduce.2.cloned.1.call-done = bf16[1024,2048]{1,0:T(8,128)(2,1)} async-done(((bf16[1024,2048]{1,0:T(8,128)(2,1)}), bf16[1024,2048]{1,0:T(8,128)(2,1)}) %all-reduce.2.cloned.1.call-update) | async-done | bytes 4194320 | tf_op jit(solution)/shard_map/psum | solution.py:116
  116.2 7.4 %fusion = (f32[1024]{0:T(1024)S(1)}, bf16[1024,2048]{1,0:T(8,128)(2,1)}) fusion(bf16[1024,2048]{1,0:T(8,128)(2,1)} %all-reduce.2.cloned.1.call-done, bf16[1024,2048]{1,0:T(8,128)(2,1)} %param.12), kind=kLoop, calls=%fused_computation.2 | loop fusion | flops 14679040 | bytes 12587008 | tf_op jit(solution)/shard_map/reduce_sum | solution.py:83
  123.6 8.4 %convolution_convert_fusion.2 = bf16[1024,1024]{0,1:T(8,128)(2,1)S(1)} fusion(bf16[2048,1024]{1,0:T(8,128)(2,1)} %all-gather.6.cloned.1.call-done, bf16[1024,2048]{1,0:T(8,128)(2,1)} %get-tuple-element.6, f32[2048]{0:T(1024)S(1)} %copy-done.6, f32[1024]{0:T(1024)S(1)} %add_rsqrt_fusion), kind=kOutput, calls=%fused_computation.29 | convolution fusion | flops 4304404480 | bytes 10498048 | tf_op jit(solution)/shard_map/dot_general | solution.py:125
  132.1 46.9 %all-gather.4.cloned.1.call-done = bf16[2048,1024]{1,0:T(8,128)(2,1)} async-done(((bf16[256,1024]{1,0:T(8,128)(2,1)}), bf16[2048,1024]{1,0:T(8,128)(2,1)}) %all-gather.4.cloned.1.call-update) | async-done | bytes 4194320 | tf_op jit(solution)/shard_map/all_gather | solution.py:121
  179.0 8.4 %convolution_convert_fusion.3 = bf16[1024,1024]{0,1:T(8,128)(2,1)S(1)} fusion(bf16[2048,1024]{1,0:T(8,128)(2,1)} %all-gather.4.cloned.1.call-done, bf16[1024,2048]{1,0:T(8,128)(2,1)} %get-tuple-element.6, f32[2048]{0:T(1024)S(1)} %copy-done.6, f32[1024]{0:T(1024)S(1)} %add_rsqrt_fusion), kind=kOutput, calls=%fused_computation.30 | convolution fusion | flops 4304404480 | bytes 10498048 | tf_op jit(solution)/shard_map/dot_general | solution.py:124
  187.9 2.5 collective-permute-start.2
  190.4 1.3 collective-permute-start.3
  191.7 2.5 pad_maximum_fusion
  194.2 22.0 %collective-permute-done.2 = bf16[1,2048]{0,1:T(8,128)(2,1)S(1)} collective-permute-done((bf16[1,2048]{0,1:T(8,128)(2,1)S(1)}, bf16[1,2048]{0,1:T(8,128)(2,1)S(1)}, u32[]{:S(2)}, u32[]{:S(2)}) %collective-permute-start.2) | collective-permute-done | bytes 4128 | tf_op jit(solution)/shard_map/ppermute | solution.py:17
  216.1 9.3 %concatenate.42 = bf16[1026,2048]{0,1:T(8,128)(2,1)} concatenate(bf16[1,2048]{0,1:T(8,128)(2,1)S(1)} %collective-permute-done.2, bf16[1024,2048]{0,1:T(8,128)(2,1)} %pad_maximum_fusion, bf16[1,2048]{0,1:T(8,128)(2,1)} %collective-permute-done.3), dimensions={0} | concatenate | bytes 8404992 | tf_op jit(solution)/shard_map/concatenate | solution.py:21
  225.5 2.9 convert_element_type.108
  228.4 8.5 %fusion.3 = f32[1024,2048]{0,1:T(8,128)} fusion(f32[1026,2048]{0,1:T(8,128)S(1)} %convert_element_type.108, f32[2048]{0:T(1024)S(1)} %bitcast.117, f32[2048]{0:T(1024)S(1)} %bitcast.116, f32[2048]{0:T(1024)S(1)} %bitcast.115), kind=kLoop, calls=%fused_computation.6 | loop fusion | flops 10485760 | bytes 33579008 | tf_op jit(solution)/shard_map/add | solution.py:130
  236.9 35.2 %all-gather.8.cloned.1.call-done = bf16[1024,2048]{1,0:T(8,128)(2,1)} async-done(((bf16[1024,256]{1,0:T(8,128)(2,1)}), bf16[1024,2048]{1,0:T(8,128)(2,1)}) %all-gather.8.cloned.1.call-update) | async-done | bytes 4194320 | tf_op jit(solution)/shard_map/all_gather | solution.py:135
  272.1 11.4 %convolution_convert_fusion.1 = bf16[1024,2048]{1,0:T(8,128)(2,1)} fusion(bf16[1024,2048]{1,0:T(8,128)(2,1)} %all-gather.8.cloned.1.call-done, f32[1024,2048]{0,1:T(8,128)} %fusion.3), kind=kOutput, calls=%fused_computation.24 | convolution fusion | flops 4303355904 | bytes 16777216 | tf_op jit(solution)/shard_map/dot_general | solution.py:134
  283.5 42.9 %reduce-scatter.2.cloned.1.call-done = bf16[256,2048]{1,0:T(8,128)(2,1)} async-done(((bf16[1024,2048]{1,0:T(8,128)(2,1)}), bf16[256,2048]{1,0:T(8,128)(2,1)}) %reduce-scatter.2.cloned.1.call-update) | async-done | bytes 1048592 | tf_op jit(solution)/shard_map/reduce_scatter | solution.py:137
  326.4 2.9 add_convert_fusion.1
  (52 shorter events, 2.3 us)
Async XLA Ops:
  7.4 18.4 %copy-start = (bf16[256,2048]{1,0:T(8,128)(2,1)S(1)}, bf16[256,2048]{1,0:T(8,128)(2,1)}, u32[]{:S(2)}) copy-start(bf16[256,2048]{1,0:T(8,128)(2,1)} %param.18) | copy-start | bytes 3145732
  7.4 12.1 %copy-start.2 = (bf16[1024,64]{0,1:T(8,128)(2,1)S(1)}, bf16[1024,64]{0,1:T(8,128)(2,1)}, u32[]{:S(2)}) copy-start(bf16[1024,64]{0,1:T(8,128)(2,1)} %param.15) | copy-start | bytes 393220
  7.4 108.8 %all-reduce.2.cloned.1.call-start = ((), (), s32[]{:S(2)}) async-start(), calls=%async_computation.1 | async-start | bytes 8388608 | tf_op jit(solution)/shard_map/psum | solution.py:116
  9.8 9.7 %collective-permute-start = (bf16[128,128]{0,1:T(8,128)(2,1)S(1)}, bf16[128,128]{0,1:T(8,128)(2,1)S(1)}, u32[]{:S(2)}, u32[]{:S(2)}) collective-permute-start(bf16[128,128]{0,1:T(8,128)(2,1)S(1)} %get-tuple-element.19), channel_id=1, source_target_pairs={{0,4},{4,8},{8,12},{12,16},{16,20},{20,24},{24,28},{1,5},{5,9},{9,... | collective-permute-start | bytes 98312 | tf_op jit(solution)/shard_map/ppermute | solution.py:17
  14.7 5.8 %collective-permute-start.1 = (bf16[128,128]{0,1:T(8,128)(2,1)S(1)}, bf16[128,128]{0,1:T(8,128)(2,1)S(1)}, u32[]{:S(2)}, u32[]{:S(2)}) collective-permute-start(bf16[128,128]{0,1:T(8,128)(2,1)S(1)} %get-tuple-element.20), channel_id=1, source_target_pairs={{4,0},{8,4},{12,8},{16,12},{20,16},{24,20},{28,24},{5,1},{9,5},{13... | collective-permute-start | bytes 98312 | tf_op jit(solution)/shard_map/ppermute | solution.py:20
  20.7 1.1 copy-start.5
  29.1 2.0 copy-start.3
  29.1 2.0 copy-start.4
  29.1 94.5 %all-gather.6.cloned.1.call-start = ((), (), s32[]{:S(2)}) async-start(), calls=%async_computation.3 | async-start | bytes 4718592 | tf_op jit(solution)/shard_map/all_gather | solution.py:122
  29.7 149.3 %all-gather.4.cloned.1.call-start = ((), (), s32[]{:S(2)}) async-start(), calls=%async_computation.2 | async-start | bytes 4718592 | tf_op jit(solution)/shard_map/all_gather | solution.py:121
  30.3 241.9 %all-gather.8.cloned.1.call-start = ((), (), s32[]{:S(2)}) async-start(), calls=%async_computation.4 | async-start | bytes 4718592 | tf_op jit(solution)/shard_map/all_gather | solution.py:135
  30.9 295.6 %reduce-scatter.2.cloned.1.call-start = ((), (), s32[]{:S(2)}) async-start(), calls=%async_computation.5 | async-start | bytes 5242880 | tf_op jit(solution)/shard_map/reduce_scatter | solution.py:137
  31.1 92.5 %copy-start.6 = (f32[2048]{0:T(1024)S(1)}, f32[2048]{0:T(1024)}, u32[]{:S(2)}) copy-start(f32[2048]{0:T(1024)} %param.17) | copy-start | bytes 24580
  187.9 28.2 %collective-permute-start.2 = (bf16[1,2048]{0,1:T(8,128)(2,1)S(1)}, bf16[1,2048]{0,1:T(8,128)(2,1)S(1)}, u32[]{:S(2)}, u32[]{:S(2)}) collective-permute-start(bf16[1,2048]{0,1:T(8,128)(2,1)S(1)} %get-tuple-element.8), channel_id=1, source_target_pairs={{0,4},{4,8},{8,12},{12,16},{16,20},{20,24},{24,28},{1,5},{5,9},{9,... | collective-permute-start | bytes 12296 | tf_op jit(solution)/shard_map/ppermute | solution.py:17
  190.4 25.7 %collective-permute-start.3 = (bf16[1,2048]{0,1:T(8,128)(2,1)S(1)}, bf16[1,2048]{0,1:T(8,128)(2,1)}, u32[]{:S(2)}, u32[]{:S(2)}) collective-permute-start(bf16[1,2048]{0,1:T(8,128)(2,1)S(1)} %get-tuple-element.7), channel_id=1, source_target_pairs={{4,0},{8,4},{12,8},{16,12},{20,16},{24,20},{28,24},{5,1},{9,5},{13... | collective-permute-start | bytes 12296 | tf_op jit(solution)/shard_map/ppermute | solution.py:20
  272.1 57.2 %copy-start.1 = (bf16[256,2048]{1,0:T(8,128)(2,1)S(1)}, bf16[256,2048]{1,0:T(8,128)(2,1)}, u32[]{:S(2)}) copy-start(bf16[256,2048]{1,0:T(8,128)(2,1)} %param.18) | copy-start | bytes 3145732
Sparse Core Ops, SparseCore 0:
  29.2 86.9 all-reduce.1
  283.7 42.7 reduce-scatter.1
Sparse Core Ops, SparseCore 1:
  31.7 74.0 all-gather.5
  107.8 71.1 all-gather.3
  180.9 91.2 all-gather.7
where the time goes:
time: 338 us; the launch traced here: 337 us
  waiting for transfers between devices  235 us (70%)
  matrix products  34.4 us (10%)
  other arithmetic  31.1 us (9%)
  between operations  15.4 us (5%)
  local copies, waits for them, and re-layouts  11.2 us (3%)
  starting transfers between devices  10.3 us (3%)
    psum x1, waiting for transfers between devices, shards(): lax.psum(partial_value.astype(jnp.bfloat16), 'tp').astype(jnp.float32)  85.1 us
    all_gather x1, waiting for transfers between devices, shards(): lax.all_gather(w_gate, 'sp', axis=0, tiled=True)  46.9 us
    reduce_scatter x1, waiting for transfers between devices, shards(): lax.psum_scatter(terms.astype(jnp.bfloat16), 'tp', scatter_dimension=0, t...  42.9 us
    all_gather x1, waiting for transfers between devices, shards(): lax.all_gather(w_down, 'sp', axis=1, tiled=True)  35.2 us
    ppermute x2, waiting for transfers between devices, extended(): lax.ppermute(lax.slice_in_dim(block, block.shape[dim] - width, None, axis...  22 us
    dot_general x1, matrix products, shards(): jnp.dot(hidden, lax.all_gather(w_down, 'sp', axis=1, tiled=True), preferr...  11.4 us
    concatenate x1, local copies, waits for them, and re-layouts, extended(): block = jnp.concatenate([low, block, high], axis=dim)  9.35 us
    add x1, other arithmetic, shards(): edged_up[:-2] * taps[0] + edged_up[1:-1] * taps[1] + edged_up[2:] * taps[2]  8.49 us
  transfers between devices with their start and end apart: 9, of which 6 were waited for; matrix products, arithmetic and copies ran while one was open for 15% of the time, Pallas kernels for 0%

commit v1 on v0

--- a/solution.py
+++ b/solution.py
@@ -113,7 +113,9 @@
         turned_query, edged[:, :key_width], edged[:, key_width:], sink, offset, total
     )
     partial_value = jnp.dot(attended, w_out, preferred_element_type=jnp.float32)
-    mix_full = lax.psum(partial_value.astype(jnp.bfloat16), "tp").astype(jnp.float32)
+    mix_full = jnp.sum(lax.all_gather(partial_value.astype(jnp.bfloat16), "tp"), axis=0).astype(
+        jnp.float32
+    )
     mid_full = (residual.astype(jnp.float32) + mix_full).astype(jnp.bfloat16)
     normed = rmsnorm(mid_full, norm_gain)
     mid_rows = lax.dynamic_slice_in_dim(mid_full, tp_index * share, share, 0)

time: 338 us -> 442 us (1.31)
  waiting for transfers between devices: 235 us -> 329 us
  other arithmetic: 31.1 us -> 43.1 us
    all_gather x0 -> x1, waiting for transfers between devices: none -> 105 us  [shards(): lax.all_gather(partial_value.astype(jnp.bfloat16), 'tp')]
    psum x1 -> x0, waiting for transfers between devices: 85.1 us -> none  [shards(): lax.psum(partial_value.astype(jnp.bfloat16), 'tp').astype(jnp.float32)]
    all_gather x1, waiting for transfers between devices: 0.01 us -> 55.3 us  [shards(): lax.all_gather(w_value, 'sp', axis=0, tiled=True)]
    all_gather x1, waiting for transfers between devices: 46.9 us -> 65.1 us  [shards(): lax.all_gather(w_gate, 'sp', axis=0, tiled=True)]
    reduce_sum x0 -> x1, other arithmetic: none -> 12.2 us  [shards(): jnp.sum(lax.all_gather(partial_value.astype(jnp.bfloat16), 'tp'), axis=0)]
  transfers between devices with their start and end apart: 9 -> 9, of which waited for: 6 -> 7; matrix products, arithmetic and copies ran while one was open for 15% -> 14% of each run, Pallas kernels for 0% -> 0%
where the time goes in v1:
time: 442 us; the launch traced here: 441 us
  waiting for transfers between devices  329 us (74%)
  other arithmetic  43.1 us (10%)
  matrix products  34.6 us (8%)
  between operations  13.5 us (3%)
  local copies, waits for them, and re-layouts  11.2 us (3%)
  starting transfers between devices  10.1 us (2%)
    all_gather x1, waiting for transfers between devices, shards(): lax.all_gather(partial_value.astype(jnp.bfloat16), 'tp')  105 us
    all_gather x1, waiting for transfers between devices, shards(): lax.all_gather(w_gate, 'sp', axis=0, tiled=True)  65.1 us
    all_gather x1, waiting for transfers between devices, shards(): lax.all_gather(w_value, 'sp', axis=0, tiled=True)  55.3 us
    reduce_scatter x1, waiting for transfers between devices, shards(): lax.psum_scatter(terms.astype(jnp.bfloat16), 'tp', scatter_dimension=0, t...  42.9 us
    all_gather x1, waiting for transfers between devices, shards(): lax.all_gather(w_down, 'sp', axis=1, tiled=True)  35.5 us
    ppermute x2, waiting for transfers between devices, extended(): lax.ppermute(lax.slice_in_dim(block, block.shape[dim] - width, None, axis...  21.9 us
    reduce_sum x1, other arithmetic, shards(): jnp.sum(lax.all_gather(partial_value.astype(jnp.bfloat16), 'tp'), axis=0)  12.2 us
    dot_general x1, matrix products, shards(): jnp.dot(hidden, lax.all_gather(w_down, 'sp', axis=1, tiled=True), preferr...  11.4 us
  transfers between devices with their start and end apart: 9, of which 7 were waited for; matrix products, arithmetic and copies ran while one was open for 14% of the time, Pallas kernels for 0%

profile of v1, /device:TPU:0, one launch (start us, length us, event | category | flops | bytes accessed | tf_op | source)
XLA Modules:
  0.0 441.4 jit_solution(7684666861331852566)
XLA Ops:
  6.6 1.0 bitcast_convert_fusion
  7.6 0.6 fusion.40
  8.2 0.7 pad_maximum_fusion.6
  9.0 4.9 %collective-permute-start = (bf16[128,128]{0,1:T(8,128)(2,1)S(1)}, bf16[128,128]{0,1:T(8,128)(2,1)S(1)}, u32[]{:S(2)}, u32[]{:S(2)}) collective-permute-start(bf16[128,128]{0,1:T(8,128)(2,1)S(1)} %get-tuple-element.19), channel_id=1, source_target_pairs={{0,4},{4,8},{8,12},{12,16},{16,20},{20,24},{24,28},{1,5},{5,9},{9,... | collective-permute-start | bytes 98312 | tf_op jit(solution)/shard_map/ppermute | solution.py:17
  13.8 1.3 collective-permute-start.1
  15.8 1.2 copy.20
  17.4 1.2 fusion.12
  18.7 0.9 collective-permute-done.1
  19.8 1.0 fusion.6
  21.0 1.5 fusion.5
  22.7 1.9 fusion.16
  25.0 3.2 convolution_convert_fusion
  28.3 0.7 all-gather.8.cloned.1.call-update
  29.0 0.7 all-gather.6.cloned.1.call-update
  30.4 105.4 %all-gather.12.cloned.1.call-done = bf16[4096,2048]{1,0:T(8,128)(2,1)} async-done(((bf16[1024,2048]{1,0:T(8,128)(2,1)}), bf16[4096,2048]{1,0:T(8,128)(2,1)}) %all-gather.12.cloned.1.call-update) | async-done | bytes 16777232 | tf_op jit(solution)/shard_map/all_gather | solution.py:116
  135.8 12.2 %reduce_sum.31 = bf16[1024,2048]{1,0:T(8,128)(2,1)} reduce(bf16[4,1024,2048]{2,1,0:T(8,128)(2,1)} %bitcast.107, bf16[]{:T(256)} %constant.44.clone.1), dimensions={0}, to_apply=%region_2.3 | reduce | flops 6291456 | bytes 20971522 | tf_op jit(solution)/shard_map/reduce_sum | solution.py:116
  148.0 7.4 %fusion = (f32[1024]{0:T(1024)S(1)}, bf16[1024,2048]{1,0:T(8,128)(2,1)}) fusion(bf16[1024,2048]{1,0:T(8,128)(2,1)} %reduce_sum.31, bf16[1024,2048]{1,0:T(8,128)(2,1)} %param.12), kind=kLoop, calls=%fused_computation.2 | loop fusion | flops 14679040 | bytes 12587008 | tf_op jit(solution)/shard_map/reduce_sum | solution.py:83
  155.4 55.3 %all-gather.8.cloned.1.call-done = bf16[2048,1024]{1,0:T(8,128)(2,1)} async-done(((bf16[256,1024]{1,0:T(8,128)(2,1)}), bf16[2048,1024]{1,0:T(8,128)(2,1)}) %all-gather.8.cloned.1.call-update) | async-done | bytes 4194320 | tf_op jit(solution)/shard_map/all_gather | solution.py:124
  210.7 8.4 %convolution_convert_fusion.2 = bf16[1024,1024]{0,1:T(8,128)(2,1)S(1)} fusion(bf16[2048,1024]{1,0:T(8,128)(2,1)} %all-gather.8.cloned.1.call-done, bf16[1024,2048]{1,0:T(8,128)(2,1)} %get-tuple-element.6, f32[2048]{0:T(1024)S(1)} %copy-done.6, f32[1024]{0:T(1024)S(1)} %add_rsqrt_fusion), kind=kOutput, calls=%fused_computation.29 | convolution fusion | flops 4304404480 | bytes 10498048 | tf_op jit(solution)/shard_map/dot_general | solution.py:127
  219.1 65.1 %all-gather.6.cloned.1.call-done = bf16[2048,1024]{1,0:T(8,128)(2,1)} async-done(((bf16[256,1024]{1,0:T(8,128)(2,1)}), bf16[2048,1024]{1,0:T(8,128)(2,1)}) %all-gather.6.cloned.1.call-update) | async-done | bytes 4194320 | tf_op jit(solution)/shard_map/all_gather | solution.py:123
  284.2 8.6 %convolution_convert_fusion.3 = bf16[1024,1024]{0,1:T(8,128)(2,1)S(1)} fusion(bf16[2048,1024]{1,0:T(8,128)(2,1)} %all-gather.6.cloned.1.call-done, bf16[1024,2048]{1,0:T(8,128)(2,1)} %get-tuple-element.6, f32[2048]{0:T(1024)S(1)} %copy-done.6, f32[1024]{0:T(1024)S(1)} %add_rsqrt_fusion), kind=kOutput, calls=%fused_computation.30 | convolution fusion | flops 4304404480 | bytes 10498048 | tf_op jit(solution)/shard_map/dot_general | solution.py:126
  293.1 2.5 collective-permute-start.2
  295.6 1.3 collective-permute-start.3
  296.9 2.6 pad_maximum_fusion
  299.5 21.9 %collective-permute-done.2 = bf16[1,2048]{0,1:T(8,128)(2,1)S(1)} collective-permute-done((bf16[1,2048]{0,1:T(8,128)(2,1)S(1)}, bf16[1,2048]{0,1:T(8,128)(2,1)S(1)}, u32[]{:S(2)}, u32[]{:S(2)}) %collective-permute-start.2) | collective-permute-done | bytes 4128 | tf_op jit(solution)/shard_map/ppermute | solution.py:17
  321.4 9.3 %concatenate.42 = bf16[1026,2048]{0,1:T(8,128)(2,1)} concatenate(bf16[1,2048]{0,1:T(8,128)(2,1)S(1)} %collective-permute-done.2, bf16[1024,2048]{0,1:T(8,128)(2,1)} %pad_maximum_fusion, bf16[1,2048]{0,1:T(8,128)(2,1)} %collective-permute-done.3), dimensions={0} | concatenate | bytes 8404992 | tf_op jit(solution)/shard_map/concatenate | solution.py:21
  330.7 2.9 convert_element_type.110
  333.7 8.5 %fusion.3 = f32[1024,2048]{0,1:T(8,128)} fusion(f32[1026,2048]{0,1:T(8,128)S(1)} %convert_element_type.110, f32[2048]{0:T(1024)S(1)} %bitcast.119, f32[2048]{0:T(1024)S(1)} %bitcast.118, f32[2048]{0:T(1024)S(1)} %bitcast.117), kind=kLoop, calls=%fused_computation.6 | loop fusion | flops 10485760 | bytes 33579008 | tf_op jit(solution)/shard_map/add | solution.py:132
  342.2 35.5 %all-gather.10.cloned.1.call-done = bf16[1024,2048]{1,0:T(8,128)(2,1)} async-done(((bf16[1024,256]{1,0:T(8,128)(2,1)}), bf16[1024,2048]{1,0:T(8,128)(2,1)}) %all-gather.10.cloned.1.call-update) | async-done | bytes 4194320 | tf_op jit(solution)/shard_map/all_gather | solution.py:137
  377.6 11.4 %convolution_convert_fusion.1 = bf16[1024,2048]{1,0:T(8,128)(2,1)} fusion(bf16[1024,2048]{1,0:T(8,128)(2,1)} %all-gather.10.cloned.1.call-done, f32[1024,2048]{0,1:T(8,128)} %fusion.3), kind=kOutput, calls=%fused_computation.24 | convolution fusion | flops 4303355904 | bytes 16777216 | tf_op jit(solution)/shard_map/dot_general | solution.py:136
  389.1 42.9 %reduce-scatter.2.cloned.1.call-done = bf16[256,2048]{1,0:T(8,128)(2,1)} async-done(((bf16[1024,2048]{1,0:T(8,128)(2,1)}), bf16[256,2048]{1,0:T(8,128)(2,1)}) %reduce-scatter.2.cloned.1.call-update) | async-done | bytes 1048592 | tf_op jit(solution)/shard_map/reduce_scatter | solution.py:139
  432.0 2.9 add_convert_fusion.1
  (53 shorter events, 2.9 us)
Async XLA Ops:
  6.5 18.4 %copy-start = (bf16[256,2048]{1,0:T(8,128)(2,1)S(1)}, bf16[256,2048]{1,0:T(8,128)(2,1)}, u32[]{:S(2)}) copy-start(bf16[256,2048]{1,0:T(8,128)(2,1)} %param.18) | copy-start | bytes 3145732
  6.5 12.1 %copy-start.2 = (bf16[1024,64]{0,1:T(8,128)(2,1)S(1)}, bf16[1024,64]{0,1:T(8,128)(2,1)}, u32[]{:S(2)}) copy-start(bf16[1024,64]{0,1:T(8,128)(2,1)} %param.15) | copy-start | bytes 393220
  6.5 129.2 %all-gather.12.cloned.1.call-start = ((), (), s32[]{:S(2)}) async-start(), calls=%async_computation.5 | async-start | bytes 20971520 | tf_op jit(solution)/shard_map/all_gather | solution.py:116
  9.0 9.7 %collective-permute-start = (bf16[128,128]{0,1:T(8,128)(2,1)S(1)}, bf16[128,128]{0,1:T(8,128)(2,1)S(1)}, u32[]{:S(2)}, u32[]{:S(2)}) collective-permute-start(bf16[128,128]{0,1:T(8,128)(2,1)S(1)} %get-tuple-element.19), channel_id=1, source_target_pairs={{0,4},{4,8},{8,12},{12,16},{16,20},{20,24},{24,28},{1,5},{5,9},{9,... | collective-permute-start | bytes 98312 | tf_op jit(solution)/shard_map/ppermute | solution.py:17
  13.8 5.8 %collective-permute-start.1 = (bf16[128,128]{0,1:T(8,128)(2,1)S(1)}, bf16[128,128]{0,1:T(8,128)(2,1)S(1)}, u32[]{:S(2)}, u32[]{:S(2)}) collective-permute-start(bf16[128,128]{0,1:T(8,128)(2,1)S(1)} %get-tuple-element.20), channel_id=1, source_target_pairs={{4,0},{8,4},{12,8},{16,12},{20,16},{24,20},{28,24},{5,1},{9,5},{13... | collective-permute-start | bytes 98312 | tf_op jit(solution)/shard_map/ppermute | solution.py:20
  19.8 1.1 copy-start.5
  28.2 2.1 copy-start.3
  28.2 2.1 copy-start.4
  28.2 182.5 %all-gather.8.cloned.1.call-start = ((), (), s32[]{:S(2)}) async-start(), calls=%async_computation.2 | async-start | bytes 4718592 | tf_op jit(solution)/shard_map/all_gather | solution.py:124
  29.0 255.2 %all-gather.6.cloned.1.call-start = ((), (), s32[]{:S(2)}) async-start(), calls=%async_computation.1 | async-start | bytes 4718592 | tf_op jit(solution)/shard_map/all_gather | solution.py:123
  29.7 347.9 %all-gather.10.cloned.1.call-start = ((), (), s32[]{:S(2)}) async-start(), calls=%async_computation.3 | async-start | bytes 4718592 | tf_op jit(solution)/shard_map/all_gather | solution.py:137
  30.3 401.7 %reduce-scatter.2.cloned.1.call-start = ((), (), s32[]{:S(2)}) async-start(), calls=%async_computation.4 | async-start | bytes 5242880 | tf_op jit(solution)/shard_map/reduce_scatter | solution.py:139
  148.0 62.7 %copy-start.6 = (f32[2048]{0:T(1024)S(1)}, f32[2048]{0:T(1024)}, u32[]{:S(2)}) copy-start(f32[2048]{0:T(1024)} %param.17) | copy-start | bytes 24580
  293.1 28.2 %collective-permute-start.2 = (bf16[1,2048]{0,1:T(8,128)(2,1)S(1)}, bf16[1,2048]{0,1:T(8,128)(2,1)S(1)}, u32[]{:S(2)}, u32[]{:S(2)}) collective-permute-start(bf16[1,2048]{0,1:T(8,128)(2,1)S(1)} %get-tuple-element.8), channel_id=1, source_target_pairs={{0,4},{4,8},{8,12},{12,16},{16,20},{20,24},{24,28},{1,5},{5,9},{9,... | collective-permute-start | bytes 12296 | tf_op jit(solution)/shard_map/ppermute | solution.py:17
  295.6 25.7 %collective-permute-start.3 = (bf16[1,2048]{0,1:T(8,128)(2,1)S(1)}, bf16[1,2048]{0,1:T(8,128)(2,1)}, u32[]{:S(2)}, u32[]{:S(2)}) collective-permute-start(bf16[1,2048]{0,1:T(8,128)(2,1)S(1)} %get-tuple-element.7), channel_id=1, source_target_pairs={{4,0},{8,4},{12,8},{16,12},{20,16},{24,20},{28,24},{5,1},{9,5},{13... | collective-permute-start | bytes 12296 | tf_op jit(solution)/shard_map/ppermute | solution.py:20
  377.6 57.2 %copy-start.1 = (bf16[256,2048]{1,0:T(8,128)(2,1)S(1)}, bf16[256,2048]{1,0:T(8,128)(2,1)}, u32[]{:S(2)}) copy-start(bf16[256,2048]{1,0:T(8,128)(2,1)} %param.18) | copy-start | bytes 3145732
Sparse Core Ops, SparseCore 0:
  28.4 107.3 all-gather.11
  137.9 72.7 all-gather.7
  212.8 71.3 all-gather.5
  286.1 91.5 all-gather.9
  389.2 42.7 reduce-scatter.1
